TPU v7x, 32 devices: a whole 2x2x4 slice. The times are simulated.
32 devices in a mesh: fs: 8 (over z, y), tp: 4 (over x, core).
Axes of the slice: x: 2, y: 2, z: 4, core: 2. Of those that a mesh axis runs over, the one named last changes fastest.
Arguments:
- tokens: bfloat16 [3072, 2048], P('fs'), may hold values from -6 to 6
- first_norm_scale: float32 [2048], replicated, may hold values from 0.1 to 1.9
- recurrent_branch_matrix: bfloat16 [2048, 1024], P('fs', 'tp'), may hold values from -0.125 to 0.125
- gelu_gate_matrix: bfloat16 [2048, 1024], P('fs', 'tp'), may hold values from -0.125 to 0.125
- filter_taps_weight: bfloat16 [4, 1024], P(None, 'tp'), may hold values from -3 to 3
- recurrence_gate_blocks: bfloat16 [16, 64, 64], P('tp'), may hold values from -0.75 to 0.75
- input_gate_blocks: bfloat16 [16, 64, 64], P('tp'), may hold values from -0.75 to 0.75
- base_decay_logits: float32 [1024], P('tp'), may hold values from 4 to 11
- extra_log_decay: float32 [3072, 1024], P('fs', 'tp'), may hold values from -0.7 to 0
- mixer_output_matrix: bfloat16 [2048, 1024], P('fs', 'tp'), may hold values from -0.5 to 0.5
- second_norm_scale: float32 [2048], replicated, may hold values from 0.1 to 1.9
- mixer_up_matrix: bfloat16 [2048, 4096], P('fs', 'tp'), may hold values from -0.125 to 0.125
- mixer_down_matrix: bfloat16 [2048, 4096], P('fs', 'tp'), may hold values from -0.09375 to 0.09375
Outputs:
- layer_out: bfloat16 [3072, 2048], P(('fs', 'tp'))
All inputs are finite; a program needn't handle non-finite values.
Results may differ from a plain program's by a relative error of at most 0.022.
Values may be sent and summed in bfloat16 or wider, within the bound.
A program may use at most 64 MiB of HBM per device.

v0:
```python
import jax
import jax.numpy as jnp
from jax import lax
from jax.sharding import PartitionSpec as P

epsilon = 1e-06
decay_rate_scale = 8.0


def rms_scaled(sequence_token_rows, scales):
    widened = sequence_token_rows.astype(jnp.float32)
    mean_square = jnp.mean(widened * widened, axis=-1, keepdims=True)
    return (widened * lax.rsqrt(mean_square + epsilon) * scales).astype(jnp.bfloat16)


def linear_combine(earlier, later):
    return (earlier[0] * later[0], later[0] * earlier[1] + later[1])


def causal_taps(branch, filter_taps_weight):
    tap_count = filter_taps_weight.shape[0]
    positions = branch.shape[0]
    padded = jnp.pad(branch.astype(jnp.float32), ((tap_count - 1, 0), (0, 0)))
    running = jnp.zeros(branch.shape, jnp.float32)
    for offset in range(tap_count):
        running = running + padded[offset : offset + positions] * filter_taps_weight[offset].astype(
            jnp.float32
        )
    return running.astype(jnp.bfloat16)


def block_map(convolved, blocks):
    positions, channels = convolved.shape
    grouped = convolved.reshape(positions, blocks.shape[0], blocks.shape[1])
    mapped = jnp.einsum("sgi,gij->sgj", grouped, blocks, preferred_element_type=jnp.float32)
    return jax.nn.sigmoid(mapped.reshape(positions, channels))


def contract_columns(left, right):
    return lax.dot_general(
        left, right, (((1,), (1,)), ((), ())), preferred_element_type=jnp.float32
    )


def local(
    tokens,
    first_norm_scale,
    recurrent_branch_matrix,
    gelu_gate_matrix,
    filter_taps_weight,
    recurrence_gate_blocks,
    input_gate_blocks,
    base_decay_logits,
    extra_log_decay,
    mixer_output_matrix,
    second_norm_scale,
    mixer_up_matrix,
    mixer_down_matrix,
):
    positions = tokens.shape[0]
    own_count = positions // lax.axis_size("tp")
    normed = rms_scaled(tokens, first_norm_scale)
    branch_sum = jnp.dot(
        normed,
        lax.all_gather(recurrent_branch_matrix, "fs", axis=0, tiled=True),
        preferred_element_type=jnp.float32,
    )
    gate_sum = jnp.dot(
        normed,
        lax.all_gather(gelu_gate_matrix, "fs", axis=0, tiled=True),
        preferred_element_type=jnp.float32,
    )
    branch = branch_sum.astype(jnp.bfloat16)
    gate_branch = gate_sum.astype(jnp.bfloat16)
    out_full = lax.all_gather(mixer_output_matrix, "fs", axis=0, tiled=True)
    convolved = causal_taps(branch, filter_taps_weight)
    recurrence_gate_value = block_map(convolved, recurrence_gate_blocks)
    admission = block_map(convolved, input_gate_blocks)
    log_keep_factor = (
        decay_rate_scale * recurrence_gate_value * jax.nn.log_sigmoid(base_decay_logits)
        + extra_log_decay
    )
    retain = jnp.exp(log_keep_factor)
    driven = jnp.sqrt(-jnp.expm1(2.0 * log_keep_factor)) * (
        admission * convolved.astype(jnp.float32)
    )
    memory = lax.associative_scan(linear_combine, (retain, driven), axis=0)[1]
    recurrent = (memory * jax.nn.gelu(gate_branch.astype(jnp.float32))).astype(jnp.bfloat16)
    up_full = lax.all_gather(mixer_up_matrix, "fs", axis=0, tiled=True)
    whole_sum = lax.psum(contract_columns(recurrent, out_full).astype(jnp.bfloat16), "tp").astype(
        jnp.float32
    )
    residual_all = (tokens.astype(jnp.float32) + whole_sum).astype(jnp.bfloat16)
    raised = jnp.dot(
        rms_scaled(residual_all, second_norm_scale), up_full, preferred_element_type=jnp.float32
    )
    hidden = jnp.square(jax.nn.relu(raised)).astype(jnp.bfloat16)
    residual = lax.dynamic_slice_in_dim(
        residual_all, lax.axis_index("tp") * own_count, own_count, 0
    )
    down_full = lax.all_gather(mixer_down_matrix, "fs", axis=0, tiled=True)
    channel_sum = lax.psum_scatter(
        contract_columns(hidden, down_full).astype(jnp.bfloat16),
        "tp",
        scatter_dimension=0,
        tiled=True,
    ).astype(jnp.float32)
    return (residual.astype(jnp.float32) + channel_sum).astype(jnp.bfloat16)


def solution(mesh):
    in_specs = (
        P("fs", None),
        P(),
        P("fs", "tp"),
        P("fs", "tp"),
        P(None, "tp"),
        P("tp", None, None),
        P("tp", None, None),
        P("tp"),
        P("fs", "tp"),
        P("fs", "tp"),
        P(),
        P("fs", "tp"),
        P("fs", "tp"),
    )
    out_specs = P(("fs", "tp"), None)
    return jax.shard_map(local, mesh=mesh, in_specs=in_specs, out_specs=out_specs, check_vma=False)
```

profile of v0, /device:TPU:0, one launch (start us, length us, event | category | flops | bytes accessed | tf_op | source)
XLA Modules:
  0.0 372.9 jit_solution(10167174261476025850)
XLA Ops:
  6.5 0.0 copy-start
  6.5 0.0 all-gather.6.cloned.1.call-start
  6.5 0.7 all-gather.6.cloned.1.call-update
  7.3 0.0 all-gather.10.cloned.1.call-start
  7.3 0.7 all-gather.10.cloned.1.call-update
  8.0 0.0 all-gather.8.cloned.1.call-start
  8.1 0.7 all-gather.8.cloned.1.call-update
  8.7 0.0 all-reduce.19.cloned.1.call-start
  8.8 0.8 slice_convert_fusion.3
  9.6 1.8 fusion.3
  11.4 0.7 fusion.59
  12.1 0.0 copy-start.3
  12.1 40.4 %all-gather.6.cloned.1.call-done = bf16[2048,256]{1,0:T(8,128)(2,1)} async-done(((bf16[256,256]{1,0:T(8,128)(2,1)}), bf16[2048,256]{1,0:T(8,128)(2,1)}) %all-gather.6.cloned.1.call-update) | async-done | bytes 1048592 | tf_op jit(solution)/shard_map/all_gather | solution.py:65
  52.5 2.3 fusion.20
  54.8 0.0 copy-start.2
  54.9 0.2 add_convert_fusion.1
  55.0 0.2 copy.20
  55.2 0.0 copy-done
  55.2 0.3 fusion.18
  55.5 0.2 copy.22
  55.7 0.0 copy-done.3
  55.7 0.3 fusion.15
  56.0 0.2 copy.24
  56.2 0.0 copy-done.2
  56.2 0.5 fusion.49
  56.7 0.1 slice.221
  56.8 0.1 slice.222
  57.0 0.1 slice.220
  57.1 0.1 slice.224
  57.2 0.1 fusion.66
  58.3 0.3 slice.278
  58.6 0.3 slice.219
  59.1 0.0 copy-start.1
  59.1 0.0 copy-start.4
  59.6 0.1 pad.69
  59.7 0.1 fusion.44
  59.7 0.1 pad.68
  59.8 33.8 %all-gather.10.cloned.1.call-done = bf16[2048,256]{1,0:T(8,128)(2,1)} async-done(((bf16[256,256]{1,0:T(8,128)(2,1)}), bf16[2048,256]{1,0:T(8,128)(2,1)}) %all-gather.10.cloned.1.call-update) | async-done | bytes 1048592 | tf_op jit(solution)/shard_map/all_gather | solution.py:75
  93.6 41.2 %all-gather.8.cloned.1.call-done = bf16[2048,256]{1,0:T(8,128)(2,1)} async-done(((bf16[256,256]{1,0:T(8,128)(2,1)}), bf16[2048,256]{1,0:T(8,128)(2,1)}) %all-gather.8.cloned.1.call-update) | async-done | bytes 1048592 | tf_op jit(solution)/shard_map/all_gather | solution.py:70
  134.8 0.0 copy-done.1
  134.8 0.0 copy-done.4
  134.8 4.6 %convolution_convert_fusion.1 = bf16[384,2048]{1,0:T(8,128)(2,1)} fusion(bf16[2048,256]{1,0:T(8,128)(2,1)} %all-gather.10.cloned.1.call-done, bf16[2048,256]{1,0:T(8,128)(2,1)} %all-gather.8.cloned.1.call-done, bf16[384,2048]{1,0:T(8,128)(2,1)S(1)} %copy-done.1, f32[2048]{0:T(1024)S(1)} %copy-done.4, f32[384]{0:T(512)S(1)} %add_rsqrt_fusion.1, ...), kind=kOutput, calls=%fused_computation.13 | convolution fusion | flops 810516480 | bytes 6039040 | tf_op jit(solution)/shard_map/dot_general | solution.py:40
  139.4 0.0 all-reduce.19.cloned.1.call-update
  139.5 0.0 copy-start.5
  139.5 0.0 all-gather.12.cloned.1.call-start
  139.5 0.5 all-gather.12.cloned.1.call-update
  140.1 0.0 all-gather.14.cloned.1.call-start
  140.1 0.5 all-gather.14.cloned.1.call-update
  140.6 0.0 reduce-scatter.2.cloned.1.call-start
  140.7 40.5 %all-reduce.19.cloned.1.call-done = bf16[384,2048]{1,0:T(8,128)(2,1)} async-done(((bf16[384,2048]{1,0:T(8,128)(2,1)}), bf16[384,2048]{1,0:T(8,128)(2,1)}) %all-reduce.19.cloned.1.call-update) | async-done | bytes 1572880 | tf_op jit(solution)/shard_map/psum | solution.py:90
  181.2 2.1 fusion
  183.3 72.7 %all-gather.12.cloned.1.call-done = bf16[2048,1024]{1,0:T(8,128)(2,1)} async-done(((bf16[256,1024]{1,0:T(8,128)(2,1)}), bf16[2048,1024]{1,0:T(8,128)(2,1)}) %all-gather.12.cloned.1.call-update) | async-done | bytes 4194320 | tf_op jit(solution)/shard_map/all_gather | solution.py:89
  256.0 73.3 %all-gather.14.cloned.1.call-done = bf16[2048,1024]{1,0:T(8,128)(2,1)} async-done(((bf16[256,1024]{1,0:T(8,128)(2,1)}), bf16[2048,1024]{1,0:T(8,128)(2,1)}) %all-gather.14.cloned.1.call-update) | async-done | bytes 4194320 | tf_op jit(solution)/shard_map/all_gather | solution.py:101
  329.4 0.0 copy-done.5
  329.4 8.1 %convolution_convert_fusion = bf16[384,2048]{1,0:T(8,128)(2,1)} fusion(bf16[2048,1024]{1,0:T(8,128)(2,1)} %all-gather.14.cloned.1.call-done, bf16[2048,1024]{1,0:T(8,128)(2,1)} %all-gather.12.cloned.1.call-done, bf16[384,2048]{1,0:T(8,128)(2,1)S(1)} %get-tuple-element.6, f32[2048]{0:T(1024)S(1)} %copy-done.5, f32[384]{0:T(512)S(1)} %add_rsqrt_fusion), kind=kOutput, calls=%fused_computation.12 | convolution fusion | flops 3226337280 | bytes 11544064 | tf_op jit(solution)/shard_map/dot_general | solution.py:40
  337.5 0.0 reduce-scatter.2.cloned.1.call-update
  337.6 26.7 %reduce-scatter.2.cloned.1.call-done = bf16[96,2048]{1,0:T(8,128)(2,1)} async-done(((bf16[384,2048]{1,0:T(8,128)(2,1)}), bf16[96,2048]{1,0:T(8,128)(2,1)}) %reduce-scatter.2.cloned.1.call-update) | async-done | bytes 393232 | tf_op jit(solution)/shard_map/reduce_scatter | solution.py:102
  364.2 1.8 add_convert_fusion
  (86 shorter events, 1.3 us)
Async XLA Ops:
  6.5 48.7 %copy-start = (bf16[4,64,64]{2,1,0:T(8,128)(2,1)S(1)}, bf16[4,64,64]{2,1,0:T(8,128)(2,1)}, u32[]{:S(2)}) copy-start(bf16[4,64,64]{2,1,0:T(8,128)(2,1)} %param.18) | copy-start | bytes 98308
  6.5 46.0 %all-gather.6.cloned.1.call-start = ((), (), s32[]{:S(2)}) async-start(), calls=%async_computation.1 | async-start | bytes 1179648 | tf_op jit(solution)/shard_map/all_gather | solution.py:65
  7.3 86.4 %all-gather.10.cloned.1.call-start = ((), (), s32[]{:S(2)}) async-start(), calls=%async_computation.3 | async-start | bytes 1179648 | tf_op jit(solution)/shard_map/all_gather | solution.py:75
  8.0 126.8 %all-gather.8.cloned.1.call-start = ((), (), s32[]{:S(2)}) async-start(), calls=%async_computation.2 | async-start | bytes 1179648 | tf_op jit(solution)/shard_map/all_gather | solution.py:70
  8.7 172.4 %all-reduce.19.cloned.1.call-start = ((), (), s32[]{:S(2)}) async-start(), calls=%async_computation.4 | async-start | bytes 3145728 | tf_op jit(solution)/shard_map/psum | solution.py:90
  12.1 43.6 %copy-start.3 = (bf16[4,64,64]{2,1,0:T(8,128)(2,1)S(1)}, bf16[4,64,64]{2,1,0:T(8,128)(2,1)}, u32[]{:S(2)}) copy-start(bf16[4,64,64]{2,1,0:T(8,128)(2,1)} %param.19) | copy-start | bytes 98308
  54.8 1.4 copy-start.2
  59.1 75.7 %copy-start.1 = (bf16[384,2048]{1,0:T(8,128)(2,1)S(1)}, bf16[384,2048]{1,0:T(8,128)(2,1)}, u32[]{:S(2)}) copy-start(bf16[384,2048]{1,0:T(8,128)(2,1)} %param.13) | copy-start | bytes 4718596
  59.1 75.7 %copy-start.4 = (f32[2048]{0:T(1024)S(1)}, f32[2048]{0:T(1024)}, u32[]{:S(2)}) copy-start(f32[2048]{0:T(1024)} %param.14) | copy-start | bytes 24580
  139.5 189.9 %copy-start.5 = (f32[2048]{0:T(1024)S(1)}, f32[2048]{0:T(1024)}, u32[]{:S(2)}) copy-start(f32[2048]{0:T(1024)} %param.23) | copy-start | bytes 24580
  139.5 116.6 %all-gather.12.cloned.1.call-start = ((), (), s32[]{:S(2)}) async-start(), calls=%async_computation.5 | async-start | bytes 4718592 | tf_op jit(solution)/shard_map/all_gather | solution.py:89
  140.1 189.3 %all-gather.14.cloned.1.call-start = ((), (), s32[]{:S(2)}) async-start(), calls=%async_computation.6 | async-start | bytes 4718592 | tf_op jit(solution)/shard_map/all_gather | solution.py:101
  140.6 223.6 %reduce-scatter.2.cloned.1.call-start = ((), (), s32[]{:S(2)}) async-start(), calls=%async_computation.7 | async-start | bytes 1966080 | tf_op jit(solution)/shard_map/reduce_scatter | solution.py:102
Sparse Core Ops, SparseCore 0:
  9.5 42.9 all-gather.5
  54.6 38.9 all-gather.9
  95.8 38.9 all-gather.7
  139.6 41.5 all-reduce.18
  183.2 72.8 all-gather.11
  258.0 71.3 all-gather.13
  337.7 26.5 reduce-scatter.1
where the time goes:
time: 373 us
  waiting for transfers between devices  332 us (89%)
  matrix products  15.7 us (4%)
  between operations  14.1 us (4%)
  other arithmetic  8.42 us (2%)
    all_gather x1, waiting for transfers between devices, local(): down_full = lax.all_gather(mixer_down_matrix, 'fs', axis=0, tiled=True)  73.3 us
    all_gather x1, waiting for transfers between devices, local(): up_full = lax.all_gather(mixer_up_matrix, 'fs', axis=0, tiled=True)  72.7 us
    all_gather x1, waiting for transfers between devices, local(): lax.all_gather(gelu_gate_matrix, 'fs', axis=0, tiled=True)  41.2 us
    psum x1, waiting for transfers between devices, local(): lax.psum(contract_columns(recurrent, out_full).astype(jnp.bfloat16), 'tp')  40.5 us
    all_gather x1, waiting for transfers between devices, local(): lax.all_gather(recurrent_branch_matrix, 'fs', axis=0, tiled=True)  40.4 us
    all_gather x1, waiting for transfers between devices, local(): out_full = lax.all_gather(mixer_output_matrix, 'fs', axis=0, tiled=True)  33.8 us
    reduce_scatter x1, waiting for transfers between devices, local(): lax.psum_scatter(contract_columns(hidden, down_full).astype(jnp.bfloat16)...  26.7 us
    dot_general x2, matrix products, contract_columns(): lax.dot_general(left, right, (((1,), (1,)), ((), ())), preferred_element_...  12.8 us
  transfers between devices with their start and end apart: 7, of which 7 were waited for; matrix products, arithmetic and copies ran while one was open for 3% of the time, Pallas kernels for 0%

commit v1 on v0

--- a/solution.py
+++ b/solution.py
@@ -1,3 +1,4 @@
+import functools
 import jax
 import jax.numpy as jnp
 from jax import lax
@@ -5,6 +6,22 @@
 
 epsilon = 1e-06
 decay_rate_scale = 8.0
+
+
+def carry_corner_in(u_in, axis_key):
+    wide_n = lax.axis_size(axis_key)
+    queue = list(map(lambda i: (i, (i + 1) % wide_n), range(wide_n)))
+
+    def extend_things(high):
+        if len(high) == wide_n:
+            return high
+        return extend_things([lax.ppermute(high[0], axis_name=axis_key, perm=queue), *high])
+
+    long_array = jnp.concatenate(extend_things([u_in]), 0)
+    return jnp.roll(long_array, (lax.axis_index(axis_key) + 1) * u_in.shape[0], 0)
+
+
+expand_the_spot = functools.partial(carry_corner_in, axis_key="fs")
 
 
 def rms_scaled(sequence_token_rows, scales):
@@ -98,7 +115,7 @@
     residual = lax.dynamic_slice_in_dim(
         residual_all, lax.axis_index("tp") * own_count, own_count, 0
     )
-    down_full = lax.all_gather(mixer_down_matrix, "fs", axis=0, tiled=True)
+    down_full = expand_the_spot(mixer_down_matrix)
     channel_sum = lax.psum_scatter(
         contract_columns(hidden, down_full).astype(jnp.bfloat16),
         "tp",

time: 373 us -> 330 us (0.88)
  waiting for transfers between devices: 332 us -> 265 us
  local copies, waits for them, and re-layouts: 2.7 us -> 25.9 us
    ppermute x0 -> x7, waiting for transfers between devices: none -> 121 us  [extend_things(): lax.ppermute(high[0], axis_name=axis_key, perm=queue)]
    all_gather x1 -> x0, waiting for transfers between devices: 73.3 us -> none  [local(): down_full = lax.all_gather(mixer_down_matrix, 'fs', axis=0, tiled=True)]
    all_gather x1, waiting for transfers between devices: 72.7 us -> 0.01 us  [local(): up_full = lax.all_gather(mixer_up_matrix, 'fs', axis=0, tiled=True)]
    psum x1, waiting for transfers between devices: 40.5 us -> 0.01 us  [local(): lax.psum(contract_columns(recurrent, out_full).astype(jnp.bfloat16), 'tp')]
    unnamed x12 -> x51, local copies, waits for them, and re-layouts: 0.03 us -> 22.4 us
  transfers between devices with their start and end apart: 7 -> 13, of which waited for: 7 -> 11; matrix products, arithmetic and copies ran while one was open for 3% -> 10% of each run, Pallas kernels for 0% -> 0%
where the time goes in v1:
time: 330 us
  waiting for transfers between devices  265 us (80%)
  local copies, waits for them, and re-layouts  25.9 us (8%)
  matrix products  15.7 us (5%)
  between operations  14.2 us (4%)
  other arithmetic  8.5 us (3%)
    ppermute x7, waiting for transfers between devices, extend_things(): lax.ppermute(high[0], axis_name=axis_key, perm=queue)  121 us
    all_gather x1, waiting for transfers between devices, local(): lax.all_gather(gelu_gate_matrix, 'fs', axis=0, tiled=True)  41.2 us
    all_gather x1, waiting for transfers between devices, local(): lax.all_gather(recurrent_branch_matrix, 'fs', axis=0, tiled=True)  40.4 us
    all_gather x1, waiting for transfers between devices, local(): out_full = lax.all_gather(mixer_output_matrix, 'fs', axis=0, tiled=True)  33.8 us
    reduce_scatter x1, waiting for transfers between devices, local(): lax.psum_scatter(contract_columns(hidden, down_full).astype(jnp.bfloat16)...  25.4 us
    unnamed x51, local copies, waits for them, and re-layouts  22.4 us
    dot_general x2, matrix products, contract_columns(): lax.dot_general(left, right, (((1,), (1,)), ((), ())), preferred_element_...  12.7 us
  transfers between devices with their start and end apart: 13, of which 11 were waited for; matrix products, arithmetic and copies ran while one was open for 10% of the time, Pallas kernels for 0%

profile of v1, /device:TPU:0, one launch (start us, length us, event | category | flops | bytes accessed | tf_op | source)
XLA Modules:
  0.0 329.7 jit_solution(18319271848752192857)
XLA Ops:
  6.5 0.7 all-gather.5.cloned.1.call-update
  7.3 0.0 all-gather.9.cloned.1.call-start
  7.3 0.7 all-gather.9.cloned.1.call-update
  8.1 0.7 all-gather.7.cloned.1.call-update
  8.7 0.0 all-reduce.19.cloned.1.call-start
  8.8 1.8 fusion.5
  10.6 0.8 slice_convert_fusion.3
  11.4 0.7 fusion.62
  12.1 40.4 %all-gather.5.cloned.1.call-done = bf16[2048,256]{1,0:T(8,128)(2,1)} async-done(((bf16[256,256]{1,0:T(8,128)(2,1)}), bf16[2048,256]{1,0:T(8,128)(2,1)}) %all-gather.5.cloned.1.call-update) | async-done | bytes 1048592 | tf_op jit(solution)/shard_map/all_gather | solution.py:82
  52.5 2.3 fusion.25
  54.9 0.2 add_convert_fusion.1
  55.0 0.2 copy.20
  55.2 0.3 fusion.23
  55.5 0.2 copy.22
  55.7 0.3 fusion.20
  56.0 0.2 copy.24
  56.2 0.5 fusion.52
  56.7 0.3 slice.219
  57.0 0.1 slice.224
  57.1 0.1 slice.220
  57.3 0.3 slice.278
  57.6 0.1 slice.222
  57.7 0.1 slice.221
  57.8 0.1 fusion.72
  59.6 0.1 fusion.47
  59.7 0.1 pad.68
  59.7 0.1 pad.69
  59.8 33.8 %all-gather.9.cloned.1.call-done = bf16[2048,256]{1,0:T(8,128)(2,1)} async-done(((bf16[256,256]{1,0:T(8,128)(2,1)}), bf16[2048,256]{1,0:T(8,128)(2,1)}) %all-gather.9.cloned.1.call-update) | async-done | bytes 1048592 | tf_op jit(solution)/shard_map/all_gather | solution.py:92
  93.6 41.2 %all-gather.7.cloned.1.call-done = bf16[2048,256]{1,0:T(8,128)(2,1)} async-done(((bf16[256,256]{1,0:T(8,128)(2,1)}), bf16[2048,256]{1,0:T(8,128)(2,1)}) %all-gather.7.cloned.1.call-update) | async-done | bytes 1048592 | tf_op jit(solution)/shard_map/all_gather | solution.py:87
  134.8 4.6 %convolution_convert_fusion = bf16[384,2048]{1,0:T(8,128)(2,1)} fusion(bf16[2048,256]{1,0:T(8,128)(2,1)} %all-gather.9.cloned.1.call-done, bf16[2048,256]{1,0:T(8,128)(2,1)} %all-gather.7.cloned.1.call-done, bf16[384,2048]{1,0:T(8,128)(2,1)S(1)} %copy-done.1, f32[2048]{0:T(1024)S(1)} %copy-done.16, f32[384]{0:T(512)S(1)} %add_rsqrt_fusion.1, ...), kind=kOutput, calls=%fused_computation.15 | convolution fusion | flops 810516480 | bytes 6039040 | tf_op jit(solution)/shard_map/dot_general | solution.py:57
  139.4 0.0 all-gather.11.cloned.1.call-start
  139.5 0.5 all-gather.11.cloned.1.call-update
  140.1 0.6 collective-permute-start
  140.7 14.1 %collective-permute-done = bf16[256,1024]{1,0:T(8,128)(2,1)S(1)} collective-permute-done((bf16[256,1024]{1,0:T(8,128)(2,1)S(1)}, bf16[256,1024]{1,0:T(8,128)(2,1)S(1)}, u32[]{:S(2)}, u32[]{:S(2)}) %collective-permute-start) | collective-permute-done | bytes 524320 | tf_op jit(solution)/shard_map/ppermute | solution.py:18
  154.8 0.8 copy-done.4
  155.6 13.8 %collective-permute-done.1 = bf16[256,1024]{1,0:T(8,128)(2,1)S(1)} collective-permute-done((bf16[256,1024]{1,0:T(8,128)(2,1)S(1)}, bf16[256,1024]{1,0:T(8,128)(2,1)S(1)}, u32[]{:S(2)}, u32[]{:S(2)}) %collective-permute-start.1) | collective-permute-done | bytes 524320 | tf_op jit(solution)/shard_map/ppermute | solution.py:18
  169.4 0.8 copy-done.6
  170.2 12.9 %collective-permute-done.2 = bf16[256,1024]{1,0:T(8,128)(2,1)S(1)} collective-permute-done((bf16[256,1024]{1,0:T(8,128)(2,1)S(1)}, bf16[256,1024]{1,0:T(8,128)(2,1)S(1)}, u32[]{:S(2)}, u32[]{:S(2)}) %collective-permute-start.2) | collective-permute-done | bytes 524320 | tf_op jit(solution)/shard_map/ppermute | solution.py:18
  183.2 0.8 copy-done.8
  184.0 12.2 %collective-permute-done.3 = bf16[256,1024]{1,0:T(8,128)(2,1)S(1)} collective-permute-done((bf16[256,1024]{1,0:T(8,128)(2,1)S(1)}, bf16[256,1024]{1,0:T(8,128)(2,1)S(1)}, u32[]{:S(2)}, u32[]{:S(2)}) %collective-permute-start.3) | collective-permute-done | bytes 524320 | tf_op jit(solution)/shard_map/ppermute | solution.py:18
  196.2 0.8 copy-done.10
  197.0 26.9 %collective-permute-done.4 = bf16[256,1024]{1,0:T(8,128)(2,1)S(1)} collective-permute-done((bf16[256,1024]{1,0:T(8,128)(2,1)S(1)}, bf16[256,1024]{1,0:T(8,128)(2,1)S(1)}, u32[]{:S(2)}, u32[]{:S(2)}) %collective-permute-start.4) | collective-permute-done | bytes 524320 | tf_op jit(solution)/shard_map/ppermute | solution.py:18
  223.9 18.0 %collective-permute-done.5 = bf16[256,1024]{1,0:T(8,128)(2,1)} collective-permute-done((bf16[256,1024]{1,0:T(8,128)(2,1)S(1)}, bf16[256,1024]{1,0:T(8,128)(2,1)}, u32[]{:S(2)}, u32[]{:S(2)}) %collective-permute-start.5) | collective-permute-done | bytes 524320 | tf_op jit(solution)/shard_map/ppermute | solution.py:18
  242.0 2.2 fusion.2
  244.3 23.3 %collective-permute-done.6 = bf16[256,1024]{1,0:T(8,128)(2,1)} collective-permute-done((bf16[256,1024]{1,0:T(8,128)(2,1)}, bf16[256,1024]{1,0:T(8,128)(2,1)}, u32[]{:S(2)}, u32[]{:S(2)}) %collective-permute-start.6) | collective-permute-done | bytes 524320 | tf_op jit(solution)/shard_map/ppermute | solution.py:18
  267.6 1.9 constant_dynamic-update-slice_fusion.15
  269.4 1.9 constant_dynamic-update-slice_fusion.14
  271.3 0.8 constant_dynamic-update-slice_fusion.13
  272.2 0.8 constant_dynamic-update-slice_fusion.12
  273.0 1.9 constant_dynamic-update-slice_fusion.11
  275.0 2.0 constant_dynamic-update-slice_fusion.10
  276.9 0.8 constant_dynamic-update-slice_fusion.9
  277.7 0.8 constant_dynamic-update-slice_fusion.8
  278.6 1.9 constant_dynamic-update-slice_fusion.7
  280.5 1.9 constant_dynamic-update-slice_fusion.6
  282.4 0.8 constant_dynamic-update-slice_fusion.5
  283.2 0.9 constant_dynamic-update-slice_fusion.4
  284.1 0.8 constant_dynamic-update-slice_fusion.3
  284.9 0.8 constant_dynamic-update-slice_fusion.2
  285.7 0.9 constant_dynamic-update-slice_fusion.1
  286.6 0.9 constant_dynamic-update-slice_fusion
  287.5 8.1 %fusion.9 = bf16[384,2048]{1,0:T(8,128)(2,1)} fusion(bf16[4096,1024]{1,0:T(8,128)(2,1)} %constant_dynamic-update-slice_fusion, s32[]{:T(128)S(6)} %select_n.24, bf16[2048,1024]{1,0:T(8,128)(2,1)} %all-gather.11.cloned.1.call-done, bf16[384,2048]{1,0:T(8,128)(2,1)S(1)} %get-tuple-element.6, f32[2048]{0:T(1024)S(1)} %copy-done.17, f32[384]{0:T(512)S(1)} %add_rsqrt_fusion), kind=kOutput, calls=%fused_computation.14 | convolution fusion | flops 3226337280 | bytes 11544068 | tf_op jit(solution)/shard_map/dot_general | solution.py:57
  295.6 25.4 %reduce-scatter.2.cloned.1.call-done = bf16[96,2048]{1,0:T(8,128)(2,1)} async-done(((bf16[384,2048]{1,0:T(8,128)(2,1)}), bf16[96,2048]{1,0:T(8,128)(2,1)}) %reduce-scatter.2.cloned.1.call-update) | async-done | bytes 393232 | tf_op jit(solution)/shard_map/reduce_scatter | solution.py:119
  321.0 1.8 add_convert_fusion
  (131 shorter events, 1.5 us)
Async XLA Ops:
  6.5 48.7 %copy-start = (bf16[4,64,64]{2,1,0:T(8,128)(2,1)S(1)}, bf16[4,64,64]{2,1,0:T(8,128)(2,1)}, u32[]{:S(2)}) copy-start(bf16[4,64,64]{2,1,0:T(8,128)(2,1)} %param.18) | copy-start | bytes 98308
  6.5 46.0 %all-gather.5.cloned.1.call-start = ((), (), s32[]{:S(2)}) async-start(), calls=%async_computation.1 | async-start | bytes 1179648 | tf_op jit(solution)/shard_map/all_gather | solution.py:82
  7.3 86.4 %all-gather.9.cloned.1.call-start = ((), (), s32[]{:S(2)}) async-start(), calls=%async_computation.3 | async-start | bytes 1179648 | tf_op jit(solution)/shard_map/all_gather | solution.py:92
  8.0 126.8 %all-gather.7.cloned.1.call-start = ((), (), s32[]{:S(2)}) async-start(), calls=%async_computation.2 | async-start | bytes 1179648 | tf_op jit(solution)/shard_map/all_gather | solution.py:87
  8.7 233.2 %all-reduce.19.cloned.1.call-start = ((), (), s32[]{:S(2)}) async-start(), calls=%async_computation.4 | async-start | bytes 3145728 | tf_op jit(solution)/shard_map/psum | solution.py:107
  10.6 45.1 %copy-start.15 = (bf16[4,64,64]{2,1,0:T(8,128)(2,1)S(1)}, bf16[4,64,64]{2,1,0:T(8,128)(2,1)}, u32[]{:S(2)}) copy-start(bf16[4,64,64]{2,1,0:T(8,128)(2,1)} %param.19) | copy-start | bytes 98308
  54.8 1.4 copy-start.14
  58.2 76.6 %copy-start.1 = (bf16[384,2048]{1,0:T(8,128)(2,1)S(1)}, bf16[384,2048]{1,0:T(8,128)(2,1)}, u32[]{:S(2)}) copy-start(bf16[384,2048]{1,0:T(8,128)(2,1)} %param.13) | copy-start | bytes 4718596
  58.2 76.6 %copy-start.16 = (f32[2048]{0:T(1024)S(1)}, f32[2048]{0:T(1024)}, u32[]{:S(2)}) copy-start(f32[2048]{0:T(1024)} %param.14) | copy-start | bytes 24580
  59.8 80.3 %copy-start.2 = (bf16[256,1024]{1,0:T(8,128)(2,1)S(1)}, bf16[256,1024]{1,0:T(8,128)(2,1)}, u32[]{:S(2)}) copy-start(bf16[256,1024]{1,0:T(8,128)(2,1)} %param.25) | copy-start | bytes 1572868
  139.4 148.1 %all-gather.11.cloned.1.call-start = ((), (), s32[]{:S(2)}) async-start(), calls=%async_computation.5 | async-start | bytes 4718592 | tf_op jit(solution)/shard_map/all_gather | solution.py:106
  140.0 181.0 %reduce-scatter.2.cloned.1.call-start = ((), (), s32[]{:S(2)}) async-start(), calls=%async_computation.6 | async-start | bytes 1966080 | tf_op jit(solution)/shard_map/reduce_scatter | solution.py:119
  140.1 14.7 %collective-permute-start = (bf16[256,1024]{1,0:T(8,128)(2,1)S(1)}, bf16[256,1024]{1,0:T(8,128)(2,1)S(1)}, u32[]{:S(2)}, u32[]{:S(2)}) collective-permute-start(bf16[256,1024]{1,0:T(8,128)(2,1)S(1)} %copy-done.2), channel_id=1, source_target_pairs={{0,4},{4,8},{8,12},{12,16},{16,20},{20,24},{24,28},{28,0},{1,5},{5... | collective-permute-start | bytes 1572872 | tf_op jit(solution)/shard_map/ppermute | solution.py:18
  154.8 0.8 copy-start.4
  155.6 13.8 %collective-permute-start.1 = (bf16[256,1024]{1,0:T(8,128)(2,1)S(1)}, bf16[256,1024]{1,0:T(8,128)(2,1)S(1)}, u32[]{:S(2)}, u32[]{:S(2)}) collective-permute-start(bf16[256,1024]{1,0:T(8,128)(2,1)S(1)} %collective-permute-done), channel_id=1, source_target_pairs={{0,4},{4,8},{8,12},{12,16},{16,20},{20,24},{24,28},{28,0},{1,5},{5... | collective-permute-start | bytes 1572872 | tf_op jit(solution)/shard_map/ppermute | solution.py:18
  169.4 0.8 copy-start.6
  170.2 12.9 %collective-permute-start.2 = (bf16[256,1024]{1,0:T(8,128)(2,1)S(1)}, bf16[256,1024]{1,0:T(8,128)(2,1)S(1)}, u32[]{:S(2)}, u32[]{:S(2)}) collective-permute-start(bf16[256,1024]{1,0:T(8,128)(2,1)S(1)} %collective-permute-done.1), channel_id=1, source_target_pairs={{0,4},{4,8},{8,12},{12,16},{16,20},{20,24},{24,28},{28,0},{1,5},{5... | collective-permute-start | bytes 1572872 | tf_op jit(solution)/shard_map/ppermute | solution.py:18
  183.2 0.8 copy-start.8
  184.0 12.2 %collective-permute-start.3 = (bf16[256,1024]{1,0:T(8,128)(2,1)S(1)}, bf16[256,1024]{1,0:T(8,128)(2,1)S(1)}, u32[]{:S(2)}, u32[]{:S(2)}) collective-permute-start(bf16[256,1024]{1,0:T(8,128)(2,1)S(1)} %collective-permute-done.2), channel_id=1, source_target_pairs={{0,4},{4,8},{8,12},{12,16},{16,20},{20,24},{24,28},{28,0},{1,5},{5... | collective-permute-start | bytes 1572872 | tf_op jit(solution)/shard_map/ppermute | solution.py:18
  196.2 0.8 copy-start.10
  197.0 26.9 %collective-permute-start.4 = (bf16[256,1024]{1,0:T(8,128)(2,1)S(1)}, bf16[256,1024]{1,0:T(8,128)(2,1)S(1)}, u32[]{:S(2)}, u32[]{:S(2)}) collective-permute-start(bf16[256,1024]{1,0:T(8,128)(2,1)S(1)} %collective-permute-done.3), channel_id=1, source_target_pairs={{0,4},{4,8},{8,12},{12,16},{16,20},{20,24},{24,28},{28,0},{1,5},{5... | collective-permute-start | bytes 1572872 | tf_op jit(solution)/shard_map/ppermute | solution.py:18
  223.9 18.1 %copy-start.12 = (bf16[256,1024]{1,0:T(8,128)(2,1)}, bf16[256,1024]{1,0:T(8,128)(2,1)S(1)}, u32[]{:S(2)}) copy-start(bf16[256,1024]{1,0:T(8,128)(2,1)S(1)} %collective-permute-done.4) | copy-start | bytes 1572868
  223.9 18.0 %collective-permute-start.5 = (bf16[256,1024]{1,0:T(8,128)(2,1)S(1)}, bf16[256,1024]{1,0:T(8,128)(2,1)}, u32[]{:S(2)}, u32[]{:S(2)}) collective-permute-start(bf16[256,1024]{1,0:T(8,128)(2,1)S(1)} %collective-permute-done.4), channel_id=1, source_target_pairs={{0,4},{4,8},{8,12},{12,16},{16,20},{20,24},{24,28},{28,0},{1,5},{5... | collective-permute-start | bytes 1572872 | tf_op jit(solution)/shard_map/ppermute | solution.py:18
  242.0 25.6 %collective-permute-start.6 = (bf16[256,1024]{1,0:T(8,128)(2,1)}, bf16[256,1024]{1,0:T(8,128)(2,1)}, u32[]{:S(2)}, u32[]{:S(2)}) collective-permute-start(bf16[256,1024]{1,0:T(8,128)(2,1)} %collective-permute-done.5), channel_id=1, source_target_pairs={{0,4},{4,8},{8,12},{12,16},{16,20},{20,24},{24,28},{28,0},{1,5},{5... | collective-permute-start | bytes 1572872 | tf_op jit(solution)/shard_map/ppermute | solution.py:18
  242.0 29.4 %copy-start.13 = (bf16[256,1024]{1,0:T(8,128)(2,1)S(1)}, bf16[256,1024]{1,0:T(8,128)(2,1)}, u32[]{:S(2)}) copy-start(bf16[256,1024]{1,0:T(8,128)(2,1)} %copy-done.12) | copy-start | bytes 1572868
  242.0 30.2 %copy-start.11 = (bf16[256,1024]{1,0:T(8,128)(2,1)S(1)}, bf16[256,1024]{1,0:T(8,128)(2,1)}, u32[]{:S(2)}) copy-start(bf16[256,1024]{1,0:T(8,128)(2,1)} %copy-done.10) | copy-start | bytes 1572868
  244.2 32.7 %copy-start.5 = (bf16[256,1024]{1,0:T(8,128)(2,1)S(1)}, bf16[256,1024]{1,0:T(8,128)(2,1)}, u32[]{:S(2)}) copy-start(bf16[256,1024]{1,0:T(8,128)(2,1)} %copy-done.4) | copy-start | bytes 1572868
  244.3 33.5 %copy-start.3 = (bf16[256,1024]{1,0:T(8,128)(2,1)S(1)}, bf16[256,1024]{1,0:T(8,128)(2,1)}, u32[]{:S(2)}) copy-start(bf16[256,1024]{1,0:T(8,128)(2,1)} %param.25) | copy-start | bytes 1572868
  273.0 11.0 %copy-start.9 = (bf16[256,1024]{1,0:T(8,128)(2,1)S(1)}, bf16[256,1024]{1,0:T(8,128)(2,1)}, u32[]{:S(2)}) copy-start(bf16[256,1024]{1,0:T(8,128)(2,1)} %copy-done.8) | copy-start | bytes 1572868
  275.0 9.9 %copy-start.7 = (bf16[256,1024]{1,0:T(8,128)(2,1)S(1)}, bf16[256,1024]{1,0:T(8,128)(2,1)}, u32[]{:S(2)}) copy-start(bf16[256,1024]{1,0:T(8,128)(2,1)} %copy-done.6) | copy-start | bytes 1572868
  278.6 8.9 %copy-start.17 = (f32[2048]{0:T(1024)S(1)}, f32[2048]{0:T(1024)}, u32[]{:S(2)}) copy-start(f32[2048]{0:T(1024)} %param.23) | copy-start | bytes 24580
Sparse Core Ops, SparseCore 0:
  9.5 42.9 all-gather.4
  54.6 38.9 all-gather.8
  95.8 38.9 all-gather.6
  139.5 41.5 all-reduce.18
  183.1 99.0 all-gather.10
  295.7 25.2 reduce-scatter.1
